TPU v7x, 32 devices: a whole 2x2x4 slice. The times are simulated.
32 devices in a mesh: st: 8 (over z, x), tp: 4 (over y, core).
Axes of the slice: x: 2, y: 2, z: 4, core: 2. Of those that a mesh axis runs over, the one named last changes fastest.
Arguments:
- tokens: bfloat16 [8192, 4096], P('st'), may hold values from -6 to 6
- passage_ids: int32 [128, 4], P('st'), may hold values from 0 to 23, as said below
- store: bfloat16 [24, 128, 4096], P('st'), may hold values from -6 to 6
- mix_gain: bfloat16 [4096], replicated, may hold values from 0.099609375 to 1.8984375
- w_query: bfloat16 [4096, 512], P(None, 'tp'), may hold values from -0.09375 to 0.09375
- w_key: bfloat16 [4096, 512], P(None, 'tp'), may hold values from -0.09375 to 0.09375
- w_value: bfloat16 [4096, 512], P(None, 'tp'), may hold values from -0.09375 to 0.09375
- w_cross_out: bfloat16 [512, 1024], P('tp'), may hold values from -0.5 to 0.5
- head_scale: float32 [4], replicated, may hold values from 1 to 4
- w_pool_in: bfloat16 [4096, 1024], P(None, 'tp'), may hold values from -0.09375 to 0.09375
- w_pool_mix: bfloat16 [4, 256, 256], replicated, may hold values from -0.375 to 0.375
- pool_scale: bfloat16 [1024], replicated, may hold values from 0.099609375 to 1.8984375
- gate_weight: float32 [1024], replicated, may hold values from -4 to 4
Outputs:
- mixed: bfloat16 [8192, 1024], P('st', 'tp')
Inputs may be any that keep to these rules, and one draw needn't show every extreme that they name: `passage_ids`: passage p is held by index p // 3 of st. The 64 ids of one index of st (its aligned blocks of rows) fall on exactly 4 owners, 16 ids on each; one owner receives 16 ids from every index of st.
All inputs are finite; a program needn't handle non-finite values.
Results may differ from a plain program's by a relative error of at most 0.013.
Values may be sent and summed in bfloat16 or wider, within the bound.
A program may use at most 128 MiB of HBM per device.

v0:
```python
import math

import jax
import jax.numpy as jnp
from jax import lax
from jax.sharding import PartitionSpec as P

HEAD_DIM = 128
GROUP_WIDTH = 256
SEQ_LEN = 128


EPSILON = 1e-06


def head_normalize(values):
    return values * lax.rsqrt(jnp.mean(values * values, axis=-1, keepdims=True) + EPSILON)


def pool_residual(pooled_in, channel_ids):
    row_count, chan_width = pooled_in.shape
    sequences = pooled_in.astype(jnp.float32).reshape(row_count // SEQ_LEN, SEQ_LEN, chan_width)
    running = jnp.cumsum(sequences, axis=1)
    padded = jnp.concatenate(
        [jnp.zeros((sequences.shape[0], 16, chan_width), jnp.float32), running], axis=1
    )
    upper_sum = padded[:, 16:]
    position = jnp.arange(SEQ_LEN)[None, :, None]
    result = jnp.zeros_like(sequences)
    for section_index in range(4):
        window = 2 << section_index
        lower_sum = padded[:, 16 - window : 16 - window + SEQ_LEN]
        counted = jnp.minimum(position + 1, window).astype(jnp.float32)
        average = (upper_sum - lower_sum) / counted
        chosen = (channel_ids // GROUP_WIDTH == section_index)[None, None, :]
        result = jnp.where(chosen, average - sequences, result)
    return result.reshape(row_count, chan_width).astype(jnp.bfloat16)


def per_device(
    tokens,
    passage_ids,
    store,
    mix_gain,
    w_query,
    w_key,
    w_value,
    w_cross_out,
    head_scale,
    w_pool_in,
    w_pool_mix,
    pool_scale,
    gate_weight,
):
    row_count = tokens.shape[0]
    floats = tokens.astype(jnp.float32)
    scaled = floats * lax.rsqrt(jnp.mean(floats * floats, axis=-1, keepdims=True) + EPSILON)
    normed = (scaled * mix_gain.astype(jnp.float32)).astype(jnp.bfloat16)
    pooled_in = jnp.dot(normed, w_pool_in, preferred_element_type=jnp.float32).astype(jnp.bfloat16)
    local_width = pooled_in.shape[1]
    tensor_rank = lax.axis_index("tp")
    offset = tensor_rank * local_width
    residual = pool_residual(pooled_in, offset + jnp.arange(local_width))
    local_groups = local_width // GROUP_WIDTH
    mix_local = lax.dynamic_slice_in_dim(w_pool_mix, tensor_rank * local_groups, local_groups, 0)
    pool_out = jnp.einsum(
        "tgc,gce->tge",
        residual.reshape(row_count, local_groups, GROUP_WIDTH),
        mix_local,
        preferred_element_type=jnp.float32,
    )
    pool_out = pool_out.reshape(row_count, local_width) * lax.dynamic_slice_in_dim(
        pool_scale, offset, local_width
    ).astype(jnp.float32)
    gate_value = jax.nn.sigmoid(
        pooled_in.astype(jnp.float32) * lax.dynamic_slice_in_dim(gate_weight, offset, local_width)
    )
    heads_local = w_query.shape[1] // HEAD_DIM
    scales = lax.dynamic_slice_in_dim(
        head_scale, tensor_rank * heads_local, heads_local
    ) / math.sqrt(HEAD_DIM)
    queries = head_normalize(
        jnp.dot(normed, w_query, preferred_element_type=jnp.float32).reshape(
            row_count, heads_local, HEAD_DIM
        )
    ).astype(jnp.bfloat16)
    owned_count, passage_len = (store.shape[0], store.shape[1])
    flat_store = store.reshape(owned_count * passage_len, store.shape[2])
    keys_own = head_normalize(
        jnp.dot(flat_store, w_key, preferred_element_type=jnp.float32).reshape(
            owned_count, passage_len, heads_local, HEAD_DIM
        )
    ).astype(jnp.bfloat16)
    values_own = (
        jnp.dot(flat_store, w_value, preferred_element_type=jnp.float32)
        .astype(jnp.bfloat16)
        .reshape(owned_count, passage_len, heads_local, HEAD_DIM)
    )
    block_count, per_block = passage_ids.shape
    block_rows = row_count // block_count
    wanted = passage_ids.reshape(-1)
    request_count = wanted.shape[0]
    st_size = lax.axis_size("st")
    capacity = (2 * request_count + st_size - 1) // st_size
    owner_rank = wanted // owned_count
    local_index = wanted % owned_count
    onehot = (owner_rank[:, None] == jnp.arange(st_size)[None, :]).astype(jnp.int32)
    order_rank = jnp.sum((jnp.cumsum(onehot, axis=0) - onehot) * onehot, axis=1)
    slot_index = owner_rank * capacity + order_rank
    requests = (
        jnp.zeros((st_size * capacity,), jnp.int32)
        .at[slot_index]
        .set(local_index)
        .reshape(st_size, capacity)
    )
    block_queries = queries.reshape(block_count, block_rows, heads_local, HEAD_DIM)
    flat_queries = block_queries.reshape(block_count, block_rows, heads_local * HEAD_DIM)
    send_rows = flat_queries[jnp.arange(request_count) // per_block]
    query_buffer = (
        jnp.zeros((st_size * capacity, block_rows, heads_local * HEAD_DIM), jnp.bfloat16)
        .at[slot_index]
        .set(send_rows)
    )
    query_buffer = query_buffer.reshape(st_size, capacity, block_rows, heads_local * HEAD_DIM)
    got_queries, asked_for = (
        lax.all_to_all(query_buffer, "st", split_axis=0, concat_axis=0, tiled=True),
        lax.all_to_all(requests, "st", split_axis=0, concat_axis=0, tiled=True),
    )
    chosen_keys = keys_own[asked_for.reshape(-1)].reshape(
        st_size, capacity, passage_len, heads_local, HEAD_DIM
    )
    chosen_values = values_own[asked_for.reshape(-1)].reshape(
        st_size, capacity, passage_len, heads_local, HEAD_DIM
    )
    got_queries = got_queries.reshape(st_size, capacity, block_rows, heads_local, HEAD_DIM)
    scores = (
        jnp.einsum(
            "scqhd,sckhd->schqk", got_queries, chosen_keys, preferred_element_type=jnp.float32
        )
        * scales[None, None, :, None, None]
    )
    weights = jnp.exp(scores)
    part_totals = jnp.transpose(jnp.sum(weights, axis=4), (0, 1, 3, 2))
    partial_out = jnp.einsum(
        "schqk,sckhd->scqhd",
        weights.astype(jnp.bfloat16),
        chosen_values,
        preferred_element_type=jnp.float32,
    )
    partial_out = partial_out.astype(jnp.bfloat16).reshape(
        st_size, capacity, block_rows, heads_local * HEAD_DIM
    )
    back_out = lax.all_to_all(partial_out, "st", split_axis=0, concat_axis=0, tiled=True)
    back_totals = lax.all_to_all(
        part_totals.astype(jnp.bfloat16), "st", split_axis=0, concat_axis=0, tiled=True
    ).astype(part_totals.dtype)
    mine_out = back_out.reshape(st_size * capacity, block_rows, heads_local, HEAD_DIM)[
        slot_index
    ].astype(jnp.float32)
    summed = jnp.sum(
        mine_out.reshape(block_count, per_block, block_rows, heads_local, HEAD_DIM), axis=1
    )
    mine_totals = back_totals.reshape(st_size * capacity, block_rows, heads_local)[slot_index]
    totals = jnp.sum(mine_totals.reshape(block_count, per_block, block_rows, heads_local), axis=1)
    attended = (
        (summed / totals[..., None]).astype(jnp.bfloat16).reshape(row_count, heads_local * HEAD_DIM)
    )
    cross_term = jnp.dot(attended, w_cross_out, preferred_element_type=jnp.float32)
    cross_sum = lax.psum_scatter(
        cross_term.astype(jnp.bfloat16), "tp", scatter_dimension=1, tiled=True
    ).astype(jnp.float32)
    return (pool_out + gate_value * cross_sum).astype(jnp.bfloat16)


def solution(mesh):
    return jax.shard_map(
        per_device,
        mesh=mesh,
        in_specs=(
            P("st", None),
            P("st", None),
            P("st", None, None),
            P(),
            P(None, "tp"),
            P(None, "tp"),
            P(None, "tp"),
            P("tp", None),
            P(),
            P(None, "tp"),
            P(),
            P(),
            P(),
        ),
        out_specs=P("st", "tp"),
        check_vma=False,
    )
```

profile of v0, /device:TPU:0, one launch (start us, length us, event | category | flops | bytes accessed | tf_op | source)
XLA Modules:
  0.0 214.5 jit_solution(2892670815326779502)
XLA Ops:
  10.9 7.3 %all-to-all-start = ((s32[8,1,16]{2,1,0:T(1,128)}), s32[8,1,16]{2,1,0:T(1,128)S(1)}, u32[]{:S(2)}, u32[]{:S(2)}) async-start(s32[8,1,16]{2,1,0:T(1,128)} %bitcast.10), calls=%async_computation | async-start | bytes 8192 | tf_op jit(solution)/shard_map/all_to_all | solution.py:127
  18.9 5.2 %fusion = f32[1024]{0:T(1024)S(1)} fusion(bf16[1024,4096]{1,0:T(8,128)(2,1)} %param.13), kind=kLoop, calls=%fused_computation.9 | loop fusion | flops 12581888 | bytes 8392704 | tf_op jit(solution)/shard_map/reduce_sum | solution.py:57
  24.6 3.7 %multiply_reduce_fusion = (f32[1024]{0:T(1024)S(1)}, f32[1024,128]{1,0:T(8,128)S(1)}) fusion(bf16[4096,128]{1,0:T(8,128)(2,1)} %param.17, bf16[1024,4096]{1,0:T(8,128)(2,1)S(1)} %copy-done.1, f32[4096]{0:T(1024)S(1)} %convert_element_type.142, f32[1024]{0:T(1024)S(1)} %add_rsqrt_fusion.1), kind=kOutput, calls=%fused_computation.55 | convolution fusion | flops 1090780160 | bytes 9986048 | tf_op jit(solution)/shard_map/dot_general | solution.py:83
  28.6 1.7 gather_fusion.1
  30.3 1.9 broadcast_in_dim.57
  32.1 9.1 %scatter_fusion = bf16[128,64,128]{2,1,0:T(8,128)(2,1)} fusion(bf16[128,64,128]{2,1,0:T(8,128)(2,1)} %broadcast_in_dim.57, s32[64]{0:T(128)S(1)} %fusion.50, bf16[64,64,128]{2,1,0:T(8,128)(2,1)} %gather_fusion.1), kind=kCustom, calls=%fused_computation.6 | custom fusion | bytes 3145984 | tf_op jit(solution)/shard_map/scatter | solution.py:122
  41.2 6.0 %all-to-all-start.1 = ((bf16[8,16,64,128]{3,2,1,0:T(8,128)(2,1)}), bf16[8,16,64,128]{3,2,1,0:T(8,128)(2,1)}, u32[]{:S(2)}, u32[]{:S(2)}) async-start(bf16[8,16,64,128]{3,2,1,0:T(8,128)(2,1)} %bitcast.82), calls=%async_computation.1 | async-start | bytes 4194304 | tf_op jit(solution)/shard_map/all_to_all | solution.py:126
  48.5 2.3 %multiply_reduce_fusion.1 = (f32[384]{0:T(512)S(1)}, f32[384,128]{1,0:T(8,128)S(1)}) fusion(bf16[384,4096]{1,0:T(8,128)(2,1)S(1)} %bitcast.78, bf16[4096,128]{1,0:T(8,128)(2,1)} %param.18), kind=kOutput, calls=%fused_computation.57 | convolution fusion | flops 402751104 | bytes 4392448 | tf_op jit(solution)/shard_map/dot_general | solution.py:90
  50.9 1.0 convolution_convert_fusion.1
  53.2 3.1 %gather_fusion.2 = bf16[128,128,128]{2,1,0:T(8,128)(2,1)} fusion(bf16[3,128,128]{2,1,0:T(8,128)(2,1)S(1)} %fusion.45, s32[1024]{0:T(1024)S(1)} %pad_clamp_fusion.1), kind=kCustom, calls=%fused_computation.2 | custom fusion | bytes 8389120 | tf_op jit(solution)/shard_map/gather | solution.py:129
  56.3 3.0 %gather_fusion = bf16[128,128,128]{2,1,0:T(8,128)(2,1)} fusion(bf16[3,128,128]{2,1,0:T(8,128)(2,1)S(1)} %bitcast.79, s32[1024]{0:T(1024)S(1)} %pad_clamp_fusion.1), kind=kCustom, calls=%fused_computation | custom fusion | bytes 8389120 | tf_op jit(solution)/shard_map/gather | solution.py:132
  59.3 35.7 %all-to-all-done.1 = bf16[8,16,64,128]{3,2,1,0:T(8,128)(2,1)} async-done(((bf16[8,16,64,128]{3,2,1,0:T(8,128)(2,1)}), bf16[8,16,64,128]{3,2,1,0:T(8,128)(2,1)}, u32[]{:S(2)}, u32[]{:S(2)}) %all-to-all-start.1) | async-done | bytes 2097184 | tf_op jit(solution)/shard_map/all_to_all | solution.py:126
  95.0 7.8 %fusion.3 = (bf16[8,16,64]{2,1,0:T(8,128)(2,1)S(1)}, f32[8,16,64,128]{3,2,1,0:T(8,128)}) fusion(f32[]{:T(128)} %bitcast.20, bf16[8,16,64,128]{3,2,1,0:T(8,128)(2,1)} %all-to-all-done.1, bf16[8,16,128,128]{3,2,1,0:T(8,128)(2,1)} %bitcast.81), kind=kOutput, calls=%fused_computation.13 | convolution fusion | flops 270524416 | bytes 10502148 | tf_op jit(solution)/shard_map/scqhd,sckhd->schqk/dot_general | solution.py:137
  103.5 3.6 %all-to-all-start.3 = ((bf16[8,2,512]{2,1,0:T(2,128)(2,1)}), bf16[8,2,512]{2,1,0:T(2,128)(2,1)S(1)}, u32[]{:S(2)}, u32[]{:S(2)}) async-start(bf16[8,2,512]{2,1,0:T(2,128)(2,1)} %reshape.498), calls=%async_computation.3 | async-start | bytes 32768 | tf_op jit(solution)/shard_map/all_to_all | solution.py:154
  107.1 6.1 %convert_bitcast_fusion = bf16[8,16,64,128]{3,2,1,0:T(8,128)(2,1)} fusion(bf16[8,16,128,128]{3,2,1,0:T(8,128)(2,1)} %bitcast.80, f32[8,16,64,128]{3,2,1,0:T(8,128)} %get-tuple-element.16, f32[]{:T(128)} %bitcast.20), kind=kOutput, calls=%fused_computation.19 | convolution fusion | flops 271581184 | bytes 10485764 | tf_op jit(solution)/shard_map/schqk,sckhd->scqhd/dot_general | solution.py:144
  113.7 5.6 %all-to-all-start.2 = ((bf16[8,16,64,128]{3,2,1,0:T(8,128)(2,1)}), bf16[8,16,64,128]{3,2,1,0:T(8,128)(2,1)}, u32[]{:S(2)}, u32[]{:S(2)}) async-start(bf16[8,16,64,128]{3,2,1,0:T(8,128)(2,1)} %convert_bitcast_fusion), calls=%async_computation.2 | async-start | bytes 4194304 | tf_op jit(solution)/shard_map/all_to_all | solution.py:153
  120.2 47.1 %all-to-all-done.2 = bf16[8,16,64,128]{3,2,1,0:T(8,128)(2,1)} async-done(((bf16[8,16,64,128]{3,2,1,0:T(8,128)(2,1)}), bf16[8,16,64,128]{3,2,1,0:T(8,128)(2,1)}, u32[]{:S(2)}, u32[]{:S(2)}) %all-to-all-start.2) | async-done | bytes 2097184 | tf_op jit(solution)/shard_map/all_to_all | solution.py:153
  167.3 3.3 %gather_fusion.3 = bf16[64,64,128]{2,1,0:T(8,128)(2,1)} fusion(bf16[128,64,128]{2,1,0:T(8,128)(2,1)} %bitcast.24, s32[1024]{0:T(1024)S(1)} %pad_clamp_fusion), kind=kCustom, calls=%fused_computation.3 | custom fusion | bytes 2097408 | tf_op jit(solution)/shard_map/gather | solution.py:157
  170.6 1.5 convert_reduce_fusion
  172.3 2.0 convolution_convert_fusion
  174.4 6.4 %fusion.20 = f32[1024,256]{1,0:T(8,128)S(1)} fusion(bf16[4096,256]{1,0:T(8,128)(2,1)} %param.22, bf16[1024,4096]{1,0:T(8,128)(2,1)} %param.13, f32[4096]{0:T(1024)S(1)} %convert_element_type.142, f32[1024]{0:T(1024)S(1)} %add_rsqrt_fusion.1), kind=kOutput, calls=%fused_computation.27 | convolution fusion | flops 2164785152 | bytes 11554816 | tf_op jit(solution)/shard_map/dot_general | solution.py:59
  181.8 2.2 %fusion.39 = bf16[8,128,256]{2,0,1:T(8,128)(2,1)S(1)} fusion(f32[8,128,256]{2,0,1:T(8,128)S(1)} %fusion.40, f32[8,128,256]{2,1,0:T(8,128)S(1)} %bitcast.85, f32[128]{0:T(128)S(1)} %get-tuple-element.21, f32[128]{0:T(128)S(1)} %get-tuple-element.22, f32[128]{0:T(128)S(1)} %get-tuple-element.23, f32[128]{0:T(128)S(1)} %get-tuple-element.24, ...), kind=kLoop, calls=%fused_computation.49 | loop fusion | flops 4456448 | bytes 2624512 | tf_op jit(solution)/shard_map/convert_element_type | solution.py:37
  186.4 18.4 %reduce-scatter.2.cloned.1.call-done = bf16[1024,256]{1,0:T(8,128)(2,1)} async-done(((bf16[1024,1024]{1,0:T(8,128)(2,1)}), bf16[1024,256]{1,0:T(8,128)(2,1)}) %reduce-scatter.2.cloned.1.call-update) | async-done | bytes 524304 | tf_op jit(solution)/shard_map/reduce_scatter | solution.py:169
  204.8 2.9 %fusion.16 = bf16[1024,256]{1,0:T(8,128)(2,1)} fusion(bf16[1024,256]{1,0:T(8,128)(2,1)} %bitcast.87, bf16[1024,256]{1,0:T(8,128)(2,1)} %reduce-scatter.2.cloned.1.call-done, f32[1024,256]{1,0:T(8,128)} %copy-done.2, f32[256]{0:T(256)S(1)} %dynamic_slice.14, f32[256]{0:T(256)S(1)} %dynamic-slice_convert_fusion, bf16[4,256,256]{2,1,0:T(8,128)(2,1)} %param.23, ...), kind=kOutput, calls=%fused_computation.25 | convolution fusion | flops 136577024 | bytes 2754564 | tf_op jit(solution)/shard_map/tgc,gce->tge/dot_general | solution.py:66
  (65 shorter events, 13.5 us)
Async XLA Ops:
  6.5 42.0 %copy-start = (bf16[3,128,4096]{2,1,0:T(8,128)(2,1)S(1)}, bf16[3,128,4096]{2,1,0:T(8,128)(2,1)}, u32[]{:S(2)}) copy-start(bf16[3,128,4096]{2,1,0:T(8,128)(2,1)} %param.15) | copy-start | bytes 9437188
  10.9 30.4 %all-to-all-start = ((s32[8,1,16]{2,1,0:T(1,128)}), s32[8,1,16]{2,1,0:T(1,128)S(1)}, u32[]{:S(2)}, u32[]{:S(2)}) async-start(s32[8,1,16]{2,1,0:T(1,128)} %bitcast.10), calls=%async_computation | async-start | bytes 8192 | tf_op jit(solution)/shard_map/all_to_all | solution.py:127
  18.9 5.8 %copy-start.1 = (bf16[1024,4096]{1,0:T(8,128)(2,1)S(1)}, bf16[1024,4096]{1,0:T(8,128)(2,1)}, u32[]{:S(2)}) copy-start(bf16[1024,4096]{1,0:T(8,128)(2,1)} %param.13) | copy-start | bytes 25165828
  32.1 15.1 %copy-start.5 = (f32[4]{0:T(128)S(1)}, f32[4]{0:T(128)}, u32[]{:S(2)}) copy-start(f32[4]{0:T(128)} %param.21) | copy-start | bytes 52
  41.2 53.8 %all-to-all-start.1 = ((bf16[8,16,64,128]{3,2,1,0:T(8,128)(2,1)}), bf16[8,16,64,128]{3,2,1,0:T(8,128)(2,1)}, u32[]{:S(2)}, u32[]{:S(2)}) async-start(bf16[8,16,64,128]{3,2,1,0:T(8,128)(2,1)} %bitcast.82), calls=%async_computation.1 | async-start | bytes 4194304 | tf_op jit(solution)/shard_map/all_to_all | solution.py:126
  47.2 3.7 %copy-start.3 = (bf16[4096,128]{1,0:T(8,128)(2,1)S(1)}, bf16[4096,128]{1,0:T(8,128)(2,1)}, u32[]{:S(2)}) copy-start(bf16[4096,128]{1,0:T(8,128)(2,1)} %param.19) | copy-start | bytes 3145732
  103.5 10.2 %all-to-all-start.3 = ((bf16[8,2,512]{2,1,0:T(2,128)(2,1)}), bf16[8,2,512]{2,1,0:T(2,128)(2,1)S(1)}, u32[]{:S(2)}, u32[]{:S(2)}) async-start(bf16[8,2,512]{2,1,0:T(2,128)(2,1)} %reshape.498), calls=%async_computation.3 | async-start | bytes 32768 | tf_op jit(solution)/shard_map/all_to_all | solution.py:154
  113.2 59.0 %copy-start.4 = (bf16[128,1024]{1,0:T(8,128)(2,1)S(1)}, bf16[128,1024]{1,0:T(8,128)(2,1)}, u32[]{:S(2)}) copy-start(bf16[128,1024]{1,0:T(8,128)(2,1)} %param.20) | copy-start | bytes 786436
  113.7 53.6 %all-to-all-start.2 = ((bf16[8,16,64,128]{3,2,1,0:T(8,128)(2,1)}), bf16[8,16,64,128]{3,2,1,0:T(8,128)(2,1)}, u32[]{:S(2)}, u32[]{:S(2)}) async-start(bf16[8,16,64,128]{3,2,1,0:T(8,128)(2,1)} %convert_bitcast_fusion), calls=%async_computation.2 | async-start | bytes 4194304 | tf_op jit(solution)/shard_map/all_to_all | solution.py:153
  119.4 85.4 %reduce-scatter.2.cloned.1.call-start = ((), (), s32[]{:S(2)}) async-start(), calls=%async_computation.5 | async-start | bytes 2621440 | tf_op jit(solution)/shard_map/reduce_scatter | solution.py:169
  180.8 1.0 copy-start.2
Sparse Core Ops, SparseCore 0:
  174.5 30.2 reduce-scatter.1
where the time goes:
time: 215 us; the launch traced here: 214 us
  waiting for transfers between devices  102 us (47%)
  matrix products  32.1 us (15%)
  local copies, waits for them, and re-layouts  29.4 us (14%)
  starting transfers between devices  22.6 us (11%)
  other arithmetic  14.4 us (7%)
  between operations  14.3 us (7%)
    all_to_all x1, waiting for transfers between devices, per_device(): lax.all_to_all(partial_out, 'st', split_axis=0, concat_axis=0, tiled=True)  47.1 us
    all_to_all x1, waiting for transfers between devices, per_device(): lax.all_to_all(query_buffer, 'st', split_axis=0, concat_axis=0, tiled=True)  35.7 us
    reduce_scatter x1, waiting for transfers between devices, per_device(): lax.psum_scatter(cross_term.astype(jnp.bfloat16), 'tp', scatter_dimension...  18.4 us
    scatter x1, local copies, waits for them, and re-layouts, per_device(): query_buffer = jnp.zeros((st_size * capacity, block_rows, heads_local * H...  9.08 us
    dot_general x1, matrix products, per_device(): jnp.einsum('scqhd,sckhd->schqk', got_queries, chosen_keys, preferred_elem...  7.79 us
    all_to_all x1, starting transfers between devices, per_device(): lax.all_to_all(requests, 'st', split_axis=0, concat_axis=0, tiled=True)  7.28 us
    dot_general x1, matrix products, per_device(): jnp.dot(normed, w_pool_in, preferred_element_type=jnp.float32)  6.36 us
    dot_general x1, matrix products, per_device(): jnp.einsum('schqk,sckhd->scqhd', weights.astype(jnp.bfloat16), chosen_val...  6.08 us
  transfers between devices with their start and end apart: 5, of which 4 were waited for; matrix products, arithmetic and copies ran while one was open for 24% of the time, Pallas kernels for 0%

commit v1 on v0

--- a/solution.py
+++ b/solution.py
@@ -98,77 +98,35 @@
     )
     block_count, per_block = passage_ids.shape
     block_rows = row_count // block_count
-    wanted = passage_ids.reshape(-1)
-    request_count = wanted.shape[0]
-    st_size = lax.axis_size("st")
-    capacity = (2 * request_count + st_size - 1) // st_size
-    owner_rank = wanted // owned_count
-    local_index = wanted % owned_count
-    onehot = (owner_rank[:, None] == jnp.arange(st_size)[None, :]).astype(jnp.int32)
-    order_rank = jnp.sum((jnp.cumsum(onehot, axis=0) - onehot) * onehot, axis=1)
-    slot_index = owner_rank * capacity + order_rank
-    requests = (
-        jnp.zeros((st_size * capacity,), jnp.int32)
-        .at[slot_index]
-        .set(local_index)
-        .reshape(st_size, capacity)
+    pair_own = jnp.concatenate([keys_own, values_own], axis=-1)
+    pair_all = lax.all_gather(pair_own, "st", axis=0, tiled=True)
+    chosen = pair_all[passage_ids.reshape(-1)].reshape(
+        block_count, per_block * passage_len, heads_local, 2 * HEAD_DIM
     )
     block_queries = queries.reshape(block_count, block_rows, heads_local, HEAD_DIM)
-    flat_queries = block_queries.reshape(block_count, block_rows, heads_local * HEAD_DIM)
-    send_rows = flat_queries[jnp.arange(request_count) // per_block]
-    query_buffer = (
-        jnp.zeros((st_size * capacity, block_rows, heads_local * HEAD_DIM), jnp.bfloat16)
-        .at[slot_index]
-        .set(send_rows)
-    )
-    query_buffer = query_buffer.reshape(st_size, capacity, block_rows, heads_local * HEAD_DIM)
-    got_queries, asked_for = (
-        lax.all_to_all(query_buffer, "st", split_axis=0, concat_axis=0, tiled=True),
-        lax.all_to_all(requests, "st", split_axis=0, concat_axis=0, tiled=True),
-    )
-    chosen_keys = keys_own[asked_for.reshape(-1)].reshape(
-        st_size, capacity, passage_len, heads_local, HEAD_DIM
-    )
-    chosen_values = values_own[asked_for.reshape(-1)].reshape(
-        st_size, capacity, passage_len, heads_local, HEAD_DIM
-    )
-    got_queries = got_queries.reshape(st_size, capacity, block_rows, heads_local, HEAD_DIM)
     scores = (
         jnp.einsum(
-            "scqhd,sckhd->schqk", got_queries, chosen_keys, preferred_element_type=jnp.float32
+            "bqhd,bkhd->bhqk",
+            block_queries,
+            chosen[..., :HEAD_DIM],
+            preferred_element_type=jnp.float32,
         )
-        * scales[None, None, :, None, None]
+        * scales[None, :, None, None]
     )
     weights = jnp.exp(scores)
-    part_totals = jnp.transpose(jnp.sum(weights, axis=4), (0, 1, 3, 2))
-    partial_out = jnp.einsum(
-        "schqk,sckhd->scqhd",
+    totals = jnp.transpose(jnp.sum(weights, axis=3), (0, 2, 1))
+    summed = jnp.einsum(
+        "bhqk,bkhd->bqhd",
         weights.astype(jnp.bfloat16),
-        chosen_values,
+        chosen[..., HEAD_DIM:],
         preferred_element_type=jnp.float32,
     )
-    partial_out = partial_out.astype(jnp.bfloat16).reshape(
-        st_size, capacity, block_rows, heads_local * HEAD_DIM
-    )
-    back_out = lax.all_to_all(partial_out, "st", split_axis=0, concat_axis=0, tiled=True)
-    back_totals = lax.all_to_all(
-        part_totals.astype(jnp.bfloat16), "st", split_axis=0, concat_axis=0, tiled=True
-    ).astype(part_totals.dtype)
-    mine_out = back_out.reshape(st_size * capacity, block_rows, heads_local, HEAD_DIM)[
-        slot_index
-    ].astype(jnp.float32)
-    summed = jnp.sum(
-        mine_out.reshape(block_count, per_block, block_rows, heads_local, HEAD_DIM), axis=1
-    )
-    mine_totals = back_totals.reshape(st_size * capacity, block_rows, heads_local)[slot_index]
-    totals = jnp.sum(mine_totals.reshape(block_count, per_block, block_rows, heads_local), axis=1)
     attended = (
         (summed / totals[..., None]).astype(jnp.bfloat16).reshape(row_count, heads_local * HEAD_DIM)
     )
-    cross_term = jnp.dot(attended, w_cross_out, preferred_element_type=jnp.float32)
-    cross_sum = lax.psum_scatter(
-        cross_term.astype(jnp.bfloat16), "tp", scatter_dimension=1, tiled=True
-    ).astype(jnp.float32)
+    cross_columns = lax.all_to_all(w_cross_out, "tp", split_axis=1, concat_axis=0, tiled=True)
+    attended_all = lax.all_gather(attended, "tp", axis=1, tiled=True)
+    cross_sum = jnp.dot(attended_all, cross_columns, preferred_element_type=jnp.float32)
     return (pool_out + gate_value * cross_sum).astype(jnp.bfloat16)
 
 

time: 215 us -> 97.2 us (0.45)
  waiting for transfers between devices: 102 us -> 30.6 us
  starting transfers between devices: 22.6 us -> 4.27 us
  local copies, waits for them, and re-layouts: 29.4 us -> 12.4 us
  matrix products: 32.1 us -> 22.4 us
    all_to_all x4 -> x1, waiting for transfers between devices: 83.3 us -> 0.01 us  [per_device(): lax.all_to_all(w_cross_out, 'tp', split_axis=1, concat_axis=0, tiled=True)]
    all_gather x0 -> x2, waiting for transfers between devices: none -> 30.5 us  [the longest x1 30.5 us: per_device(): pair_all = lax.all_gather(pair_own, 'st', axis=0, tiled=True)]
    reduce_scatter x1 -> x0, waiting for transfers between devices: 18.4 us -> none  [per_device(): lax.psum_scatter(cross_term.astype(jnp.bfloat16), 'tp', scatter_dimension...]
    all_to_all x4 -> x1, starting transfers between devices: 22.6 us -> 4.27 us  [per_device(): lax.all_to_all(w_cross_out, 'tp', split_axis=1, concat_axis=0, tiled=True)]
    dot_general x3, matrix products: 15.9 us -> 5.95 us  [the longest x1 2.67 us: per_device(): jnp.einsum('bqhd,bkhd->bhqk', block_queries, chosen[..., :HEAD_DIM], pref...]
    scatter x2 -> x0, local copies, waits for them, and re-layouts: 9.86 us -> none  [the longest x1 9.08 us: per_device(): query_buffer = jnp.zeros((st_size * capacity, block_rows, heads_local * H...]
    gather x5 -> x1, local copies, waits for them, and re-layouts: 11.6 us -> 4.17 us  [per_device(): pair_all[passage_ids.reshape(-1)]]
  transfers between devices with their start and end apart: 5 -> 3, of which waited for: 4 -> 1; matrix products, arithmetic and copies ran while one was open for 24% -> 38% of each run, Pallas kernels for 0% -> 0%
where the time goes in v1:
time: 97.2 us; the launch traced here: 96.6 us
  waiting for transfers between devices  30.6 us (31%)
  matrix products  22.4 us (23%)
  between operations  14.2 us (15%)
  other arithmetic  12.8 us (13%)
  local copies, waits for them, and re-layouts  12.4 us (13%)
  starting transfers between devices  4.27 us (4%)
    all_gather x1, waiting for transfers between devices, per_device(): pair_all = lax.all_gather(pair_own, 'st', axis=0, tiled=True)  30.5 us
    dot_general x1, matrix products, per_device(): jnp.dot(normed, w_pool_in, preferred_element_type=jnp.float32)  7.38 us
    reduce_sum x1, other arithmetic, per_device(): jnp.mean(floats * floats, axis=-1, keepdims=True) + EPSILON  5.25 us
    all_to_all x1, starting transfers between devices, per_device(): lax.all_to_all(w_cross_out, 'tp', split_axis=1, concat_axis=0, tiled=True)  4.27 us
    gather x1, local copies, waits for them, and re-layouts, per_device(): pair_all[passage_ids.reshape(-1)]  4.17 us
    convert_element_type x1, other arithmetic, pool_residual(): return result.reshape(row_count, chan_width).astype(jnp.bfloat16)  3.81 us
    dot_general x1, matrix products, per_device(): jnp.dot(normed, w_query, preferred_element_type=jnp.float32)  3.75 us
    unnamed x20, local copies, waits for them, and re-layouts  3.69 us
  transfers between devices with their start and end apart: 3, of which 1 were waited for; matrix products, arithmetic and copies ran while one was open for 38% of the time, Pallas kernels for 0%

profile of v1, /device:TPU:0, one launch (start us, length us, event | category | flops | bytes accessed | tf_op | source)
XLA Modules:
  0.0 96.6 jit_solution(4386939071380454417)
XLA Ops:
  6.5 1.9 %copy-done = bf16[3,128,4096]{2,1,0:T(8,128)(2,1)S(1)} copy-done((bf16[3,128,4096]{2,1,0:T(8,128)(2,1)S(1)}, bf16[3,128,4096]{2,1,0:T(8,128)(2,1)}, u32[]{:S(2)}) %copy-start) | copy-done | bytes 3145752
  8.4 2.4 %multiply_reduce_fusion.1 = (f32[384]{0:T(512)S(1)}, f32[384,128]{1,0:T(8,128)S(1)}) fusion(bf16[384,4096]{1,0:T(8,128)(2,1)S(1)} %bitcast.68, bf16[4096,128]{1,0:T(8,128)(2,1)} %param.18), kind=kOutput, calls=%fused_computation.54 | convolution fusion | flops 402751104 | bytes 4392448 | tf_op jit(solution)/shard_map/dot_general | solution.py:90
  10.9 1.0 %convolution_convert_fusion = bf16[384,128]{1,0:T(8,128)(2,1)S(1)} fusion(bf16[384,4096]{1,0:T(8,128)(2,1)S(1)} %bitcast.69, bf16[4096,128]{1,0:T(8,128)(2,1)S(1)} %copy-done.4), kind=kOutput, calls=%fused_computation.27 | convolution fusion | flops 402702336 | bytes 4292608 | tf_op jit(solution)/shard_map/dot_general | solution.py:95
  12.0 0.7 pad_maximum_fusion
  12.7 0.8 copy.49
  13.6 4.3 %all-to-all-start = ((bf16[128,4,256]{0,2,1:T(8,128)(2,1)}), bf16[128,4,256]{0,2,1:T(8,128)(2,1)}, u32[]{:S(2)}, u32[]{:S(2)}) async-start(bf16[128,4,256]{0,2,1:T(8,128)(2,1)} %bitcast.22), calls=%async_computation | async-start | bytes 524288 | tf_op jit(solution)/shard_map/all_to_all | solution.py:127
  18.0 0.6 dynamic_slice.15
  19.3 5.2 %fusion = f32[1024]{0:T(1024)S(1)} fusion(bf16[1024,4096]{1,0:T(8,128)(2,1)} %param.13), kind=kLoop, calls=%fused_computation.3 | loop fusion | flops 12581888 | bytes 8392704 | tf_op jit(solution)/shard_map/reduce_sum | solution.py:57
  24.6 0.7 copy-done.2
  25.3 3.8 %multiply_reduce_fusion = (f32[1024]{0:T(1024)S(1)}, f32[1024,128]{1,0:T(8,128)S(1)}) fusion(bf16[4096,128]{1,0:T(8,128)(2,1)} %param.17, bf16[1024,4096]{1,0:T(8,128)(2,1)S(1)} %copy-done.2, f32[4096]{0:T(1024)S(1)} %convert_element_type.91, f32[1024]{0:T(1024)S(1)} %add_rsqrt_fusion.1), kind=kOutput, calls=%fused_computation.51 | convolution fusion | flops 1090780160 | bytes 9986048 | tf_op jit(solution)/shard_map/dot_general | solution.py:83
  29.1 0.2 multiply_convert_fusion
  29.3 30.5 %all-gather.3.cloned.1.call-done = bf16[24,128,1,256]{3,1,2,0:T(8,128)(2,1)} async-done(((bf16[3,128,1,256]{3,1,2,0:T(8,128)(2,1)}), bf16[24,128,1,256]{3,1,2,0:T(8,128)(2,1)}) %all-gather.3.cloned.1.call-update) | async-done | bytes 1572880 | tf_op jit(solution)/shard_map/all_gather | solution.py:102
  59.8 4.2 %gather_fusion = bf16[64,128,256]{2,1,0:T(8,128)(2,1)} fusion(bf16[24,128,256]{2,1,0:T(8,128)(2,1)} %bitcast.70, s32[1024]{0:T(1024)S(1)} %pad_clamp_fusion), kind=kCustom, calls=%fused_computation | custom fusion | bytes 8388864 | tf_op jit(solution)/shard_map/gather | solution.py:103
  63.9 2.7 %fusion.9 = (f32[16,64]{1,0:T(8,128)S(1)}, f32[16,64,512]{2,1,0:T(8,128)S(1)}) fusion(f32[]{:T(128)} %bitcast.18, bf16[16,64,128]{2,1,0:T(8,128)(2,1)S(1)} %bitcast.76, bf16[16,512,1,256]{3,1,0,2:T(8,128)(2,1)} %bitcast.71), kind=kOutput, calls=%fused_computation.13 | convolution fusion | flops 135265280 | bytes 4461056 | tf_op jit(solution)/shard_map/bqhd,bkhd->bhqk/dot_general | solution.py:108
  66.8 1.3 %fusion.43 = bf16[16,1,128,64]{2,3,0,1:T(8,128)(2,1)} fusion(bf16[16,512,1,256]{3,1,0,2:T(8,128)(2,1)S(1)} %bitcast.72, f32[16,64,512]{2,1,0:T(8,128)S(1)} %get-tuple-element.10, f32[]{:T(128)} %bitcast.18, f32[16,64]{1,0:T(8,128)S(1)} %get-tuple-element.9), kind=kOutput, calls=%fused_computation.47 | convolution fusion | flops 135528448 | bytes 4464644 | tf_op jit(solution)/shard_map/bhqk,bkhd->bqhd/dot_general | solution.py:118
  68.0 7.4 %fusion.17 = f32[1024,256]{1,0:T(8,128)} fusion(bf16[4096,256]{1,0:T(8,128)(2,1)} %param.22, bf16[1024,4096]{1,0:T(8,128)(2,1)} %param.13, f32[4096]{0:T(1024)S(1)} %convert_element_type.91, f32[1024]{0:T(1024)S(1)} %add_rsqrt_fusion.1), kind=kOutput, calls=%fused_computation.21 | convolution fusion | flops 2164785152 | bytes 11554816 | tf_op jit(solution)/shard_map/dot_general | solution.py:59
  75.5 1.8 %fusion.46 = f32[8,128,256]{2,0,1:T(8,128)S(1)} fusion(f32[8,128,256]{2,1,0:T(8,128)} %bitcast.73), kind=kOutput, calls=%fused_computation.48 | output fusion | flops 33292288 | bytes 2097152 | tf_op jit(solution)/shard_map/jit(cumsum)/reduce_window_sum | solution.py:23
  77.3 3.8 %fusion.39 = bf16[8,128,256]{2,0,1:T(8,128)(2,1)} fusion(f32[8,128,256]{2,0,1:T(8,128)S(1)} %fusion.46, f32[8,128,256]{2,1,0:T(8,128)} %bitcast.74, f32[128]{0:T(128)S(1)} %get-tuple-element.15, f32[128]{0:T(128)S(1)} %get-tuple-element.16, f32[128]{0:T(128)S(1)} %get-tuple-element.17, f32[128]{0:T(128)S(1)} %get-tuple-element.18, ...), kind=kLoop, calls=%fused_computation.45 | loop fusion | flops 4456448 | bytes 2624512 | tf_op jit(solution)/shard_map/convert_element_type | solution.py:37
  81.1 2.0 %copy.44 = bf16[8,128,256]{2,1,0:T(8,128)(2,1)} copy(bf16[8,128,256]{2,0,1:T(8,128)(2,1)} %fusion.39) | data formatting | bytes 1048576 | tf_op jit(solution)/shard_map/convert_element_type | solution.py:37
  83.1 0.8 dynamic_slice.14
  83.8 0.8 dynamic-slice_convert_fusion
  84.6 1.1 %copy.50 = bf16[4,128,256]{2,1,0:T(8,128)(2,1)S(1)} copy(bf16[4,128,256]{1,2,0:T(8,128)(2,1)} %bitcast.23) | data formatting | bytes 524288 | tf_op jit(solution)/shard_map/all_to_all | solution.py:127
  85.7 2.0 %convolution_multiply_fusion = f32[1024,256]{1,0:T(8,128)S(1)} fusion(bf16[1024,512]{1,0:T(8,128)(2,1)} %all-gather.5.cloned.1.call-done, bf16[512,256]{1,0:T(8,128)(2,1)S(1)} %bitcast.80, f32[1024,256]{1,0:T(8,128)} %fusion.17, f32[256]{0:T(256)S(1)} %dynamic_slice.14), kind=kOutput, calls=%fused_computation.18 | convolution fusion | flops 269746176 | bytes 3408896 | tf_op jit(solution)/shard_map/dot_general | solution.py:129
  87.8 2.0 %fusion.13 = bf16[1024,256]{1,0:T(8,128)(2,1)} fusion(f32[1024,256]{1,0:T(8,128)S(1)} %convolution_multiply_fusion, bf16[1024,256]{1,0:T(8,128)(2,1)S(1)} %bitcast.75, f32[256]{0:T(256)S(1)} %dynamic-slice_convert_fusion, bf16[4,256,256]{2,1,0:T(8,128)(2,1)} %param.23, s32[]{:T(128)S(6)} %select_n.52), kind=kOutput, calls=%fused_computation.19 | convolution fusion | flops 135004160 | bytes 2229252 | tf_op jit(solution)/shard_map/tgc,gce->tge/dot_general | solution.py:66
  (35 shorter events, 0.6 us)
Async XLA Ops:
  6.5 1.9 %copy-start = (bf16[3,128,4096]{2,1,0:T(8,128)(2,1)S(1)}, bf16[3,128,4096]{2,1,0:T(8,128)(2,1)}, u32[]{:S(2)}) copy-start(bf16[3,128,4096]{2,1,0:T(8,128)(2,1)} %param.15) | copy-start | bytes 9437188
  6.5 53.2 %all-gather.3.cloned.1.call-start = ((), (), s32[]{:S(2)}) async-start(), calls=%async_computation.1 | async-start | bytes 1769472 | tf_op jit(solution)/shard_map/all_gather | solution.py:102
  8.4 2.4 %copy-start.4 = (bf16[4096,128]{1,0:T(8,128)(2,1)S(1)}, bf16[4096,128]{1,0:T(8,128)(2,1)}, u32[]{:S(2)}) copy-start(bf16[4096,128]{1,0:T(8,128)(2,1)} %param.19) | copy-start | bytes 3145732
  8.4 4.3 %copy-start.5 = (bf16[128,1024]{1,0:T(8,128)(2,1)S(1)}, bf16[128,1024]{1,0:T(8,128)(2,1)}, u32[]{:S(2)}) copy-start(bf16[128,1024]{1,0:T(8,128)(2,1)} %param.20) | copy-start | bytes 786436
  10.8 7.0 %copy-start.7 = (s32[16,4]{0,1:T(4,128)S(1)}, s32[16,4]{0,1:T(4,128)}, u32[]{:S(2)}) copy-start(s32[16,4]{0,1:T(4,128)} %param.14) | copy-start | bytes 772
  10.8 7.2 %copy-start.6 = (bf16[4096]{0:T(1024)(128)(2,1)S(1)}, bf16[4096]{0:T(1024)(128)(2,1)}, u32[]{:S(2)}) copy-start(bf16[4096]{0:T(1024)(128)(2,1)} %param.16) | copy-start | bytes 24580
  10.8 7.2 %copy-start.8 = (f32[4]{0:T(128)S(1)}, f32[4]{0:T(128)}, u32[]{:S(2)}) copy-start(f32[4]{0:T(128)} %param.21) | copy-start | bytes 52
  13.6 71.0 %all-to-all-start = ((bf16[128,4,256]{0,2,1:T(8,128)(2,1)}), bf16[128,4,256]{0,2,1:T(8,128)(2,1)}, u32[]{:S(2)}, u32[]{:S(2)}) async-start(bf16[128,4,256]{0,2,1:T(8,128)(2,1)} %bitcast.22), calls=%async_computation | async-start | bytes 524288 | tf_op jit(solution)/shard_map/all_to_all | solution.py:127
  17.8 67.9 %all-gather.5.cloned.1.call-start = ((), (), s32[]{:S(2)}) async-start(), calls=%async_computation.2 | async-start | bytes 1310720 | tf_op jit(solution)/shard_map/all_gather | solution.py:128
  19.3 6.0 %copy-start.2 = (bf16[1024,4096]{1,0:T(8,128)(2,1)S(1)}, bf16[1024,4096]{1,0:T(8,128)(2,1)}, u32[]{:S(2)}) copy-start(bf16[1024,4096]{1,0:T(8,128)(2,1)} %param.13) | copy-start | bytes 25165828
  63.9 2.8 %copy-start.1 = (bf16[64,128,256]{2,1,0:T(8,128)(2,1)S(1)}, bf16[64,128,256]{2,1,0:T(8,128)(2,1)}, u32[]{:S(2)}) copy-start(bf16[64,128,256]{2,1,0:T(8,128)(2,1)} %gather_fusion) | copy-start | bytes 12582916
  85.7 2.0 %copy-start.3 = (bf16[8,128,256]{2,1,0:T(8,128)(2,1)S(1)}, bf16[8,128,256]{2,1,0:T(8,128)(2,1)}, u32[]{:S(2)}) copy-start(bf16[8,128,256]{2,1,0:T(8,128)(2,1)} %copy.44) | copy-start | bytes 1572868
Sparse Core Ops, SparseCore 0:
  12.8 46.9 all-gather.2
  68.2 15.1 all-gather.4

commit v2 on v1

v2 whole, which is shorter than its diff:
```python
import functools
import math

import jax
import jax.numpy as jnp
from jax import lax
from jax.experimental import pallas as pl
from jax.experimental.pallas import tpu as pltpu
from jax.sharding import PartitionSpec as P

MESH = pl.DeviceIdType.MESH
SEQ_LEN = 128
EPSILON = 1e-06
TILE = 256
F32 = jnp.float32
BF16 = jnp.bfloat16


def kernel(
    n,
    tp_size,
    tok_h,
    ids_s,
    store_h,
    gain_v,
    wq_h,
    wk_h,
    wv_h,
    wc_h,
    hs_s,
    wp_h,
    mix_h,
    ps_v,
    gw_v,
    out_v,
    tok,
    store,
    wkv,
    wqp,
    mix,
    wc,
    kv,
    xg,
    rs,
    q,
    pool,
    gate,
    num,
    tot,
    att,
    local_sem,
    tok_sem,
    store_sem,
    wc_send,
    wc_recv,
    kv_send,
    kv_recv,
    att_send,
    att_recv,
    *,
    hd,
):
    st = lax.axis_index("st")
    tp = lax.axis_index("tp")
    half_n = n // 2
    owned, p_len, depth = store.shape
    rows = tok.shape[0]
    tiles = rows // TILE
    width = mix.shape[0]
    blocks, per_block = ids_s.shape
    block_rows = rows // blocks
    tile_blocks = TILE // block_rows
    half_rows = p_len // 2

    pos = jnp.where(lax.rem(st, 2) == 0, st // 2, n - 1 - st // 2)

    def ring_id(p):
        p = lax.rem(p + 2 * n, n)
        return jnp.where(p < half_n, 2 * p, 2 * (n - 1 - p) + 1)

    right = {"st": ring_id(pos + 1)}
    left = {"st": ring_id(pos - 1)}
    core_mate = tp + 1 - 2 * lax.rem(tp, 2)
    far_mate = lax.rem(tp + 2, tp_size)
    far_core = lax.rem(core_mate + 2, tp_size)

    barrier = pltpu.get_barrier_semaphore()
    for target in (right, left, {"tp": core_mate}, {"tp": far_mate}, {"tp": far_core}):
        pl.semaphore_signal(barrier, inc=1, device_id=target, device_id_type=MESH)

    wk_copy = pltpu.make_async_copy(wk_h, wkv.at[:, 0:hd], local_sem.at[0])
    wv_copy = pltpu.make_async_copy(wv_h, wkv.at[:, hd : 2 * hd], local_sem.at[1])
    wk_copy.start()
    wv_copy.start()
    store_copies = [
        pltpu.make_async_copy(store_h.at[i], store.at[i], store_sem.at[i]) for i in range(owned)
    ]
    for copy in store_copies:
        copy.start()
    wq_copy = pltpu.make_async_copy(wq_h, wqp.at[:, 0:hd], local_sem.at[2])
    wp_copy = pltpu.make_async_copy(wp_h, wqp.at[:, hd : hd + width], local_sem.at[3])
    mix_copy = pltpu.make_async_copy(mix_h.at[tp], mix, local_sem.at[4])
    wq_copy.start()
    wp_copy.start()

    def tok_copy(t):
        part = pl.ds(pl.multiple_of(t * TILE, TILE), TILE)
        return pltpu.make_async_copy(tok_h.at[part], tok.at[part], tok_sem.at[t])

    for t in range(tiles):
        tok_copy(t).start()
    mix_copy.start()

    def columns_of(index):
        return wc_h.at[:, pl.ds(pl.multiple_of(index * width, width), width)]

    wc_copy = pltpu.make_async_copy(columns_of(tp), wc.at[tp], local_sem.at[5])
    wc_copy.start()

    def wc_remote(k, mate, slot):
        return pltpu.make_async_remote_copy(
            src_ref=columns_of(mate),
            dst_ref=wc.at[slot],
            send_sem=wc_send.at[k],
            recv_sem=wc_recv.at[k],
            device_id={"tp": mate},
            device_id_type=MESH,
        )

    mates = (core_mate, far_mate, far_core)

    def piece(way, step, i, half):
        origin = ring_id(pos - (step - 1)) if way == 0 else ring_id(pos + (step - 1))
        ref = kv.at[origin, i]
        if half:
            ref = kv.at[origin, i, pl.ds(way * half_rows, half_rows)]
        return pltpu.make_async_remote_copy(
            src_ref=ref,
            dst_ref=ref,
            send_sem=kv_send.at[way, step - 1, i],
            recv_sem=kv_recv.at[way, step - 1, i],
            device_id=right if way == 0 else left,
            device_id_type=MESH,
        )

    def arrived(way, step, i, half):
        origin = ring_id(pos - step) if way == 0 else ring_id(pos + step)
        ref = kv.at[origin, i]
        if half:
            ref = kv.at[origin, i, pl.ds(way * half_rows, half_rows)]
        pltpu.make_async_remote_copy(
            src_ref=ref,
            dst_ref=ref,
            send_sem=kv_send.at[way, step - 1, i],
            recv_sem=kv_recv.at[way, step - 1, i],
            device_id=right if way == 0 else left,
            device_id_type=MESH,
        ).wait_recv()

    def head_normal(values):
        return values * lax.rsqrt(jnp.mean(values * values, axis=-1, keepdims=True) + EPSILON)

    wk_copy.wait()
    wv_copy.wait()
    for i in range(owned):
        store_copies[i].wait()
        both = jnp.dot(store[i], wkv[...], preferred_element_type=F32)
        kv[st, i, :, 0:hd] = head_normal(both[:, 0:hd]).astype(BF16)
        kv[st, i, :, hd : 2 * hd] = both[:, hd : 2 * hd].astype(BF16)
        if i == 0:
            pl.semaphore_wait(barrier, 5)
        piece(0, 1, i, False).start()
        piece(1, 1, i, False).start()
    for k in range(3):
        wc_remote(k, mates[k], tp).start()

    def tick(step, i, forward_half):
        for way in (0, 1):
            arrived(way, step, i, False)
            piece(way, step + 1, i, forward_half).start()

    wq_copy.wait()
    wp_copy.wait()
    mix_copy.wait()
    window = jnp.left_shift(2, tp)
    row_at = lax.broadcasted_iota(jnp.int32, (SEQ_LEN, SEQ_LEN), 0)
    col_at = lax.broadcasted_iota(jnp.int32, (SEQ_LEN, SEQ_LEN), 1)
    gap = row_at - col_at
    band = jnp.where((gap >= 0) & (gap < window), 1.0, 0.0).astype(BF16)
    position = lax.broadcasted_iota(jnp.int32, (SEQ_LEN, width), 0)
    counted = jnp.minimum(position + 1, window).astype(F32)
    strip = 32

    def token_tile(t, carry):
        tok_copy(t).wait()

        def norm_strip(u, carry):
            inner = pl.ds(pl.multiple_of(u * strip, strip), strip)
            x = tok[pl.ds(pl.multiple_of(t * TILE + u * strip, strip), strip), :]
            xf = x.astype(F32)
            square = jnp.mean(xf * xf, axis=-1, keepdims=True)
            rs[inner, :] = jnp.broadcast_to(lax.rsqrt(square + EPSILON), (strip, 128))
            xg[inner, :] = (xf * gain_v[...]).astype(BF16)
            return carry

        lax.fori_loop(0, TILE // strip, norm_strip, 0)
        part = pl.ds(pl.multiple_of(t * TILE, TILE), TILE)
        scale_row = rs[:, 0:1]
        projected = jnp.dot(xg[...], wqp[...], preferred_element_type=F32) * scale_row
        q[part, :] = head_normal(projected[:, 0:hd]).astype(BF16)
        pooled = projected[:, hd : hd + width].astype(BF16)
        for sequence in range(TILE // SEQ_LEN):
            part_in = pooled[sequence * SEQ_LEN : (sequence + 1) * SEQ_LEN]
            values = part_in.astype(F32)
            sums = jnp.dot(band, part_in, preferred_element_type=F32)
            residual = (sums / counted - values).astype(BF16)
            place = pl.ds(
                pl.multiple_of(t * TILE + sequence * SEQ_LEN, SEQ_LEN), SEQ_LEN
            )
            mixed = jnp.dot(residual, mix[...], preferred_element_type=F32)
            pool[place, :] = mixed * ps_v[tp].astype(F32)
            gate[place, :] = jax.nn.sigmoid(values * gw_v[tp])
        num[part, :] = jnp.zeros((TILE, hd), F32)
        tot[part, :] = jnp.zeros((TILE, p_len), F32)

        @pl.when(t >= tiles - owned)
        def _():
            tick(1, t - (tiles - owned), False)

        return carry

    lax.fori_loop(0, tiles, token_tile, 0)

    head_factor = hs_s[tp] / math.sqrt(hd)

    def attend(t, sources):
        part = pl.ds(pl.multiple_of(t * TILE, TILE), TILE)
        keys = jnp.concatenate([kv[o, i, :, 0:hd] for o, i in sources], axis=0)
        vals = jnp.concatenate([kv[o, i, :, hd : 2 * hd] for o, i in sources], axis=0)
        scores = lax.dot_general(
            q[part, :], keys, (((1,), (1,)), ((), ())), preferred_element_type=F32
        )
        weights = jnp.exp(scores * head_factor)
        parts = []
        total = None
        for k, (o, i) in enumerate(sources):
            wanted = o * owned + i
            bands = []
            for b in range(tile_blocks):
                count = jnp.int32(0)
                for j in range(per_block):
                    apart = ids_s[t * tile_blocks + b, j] - wanted
                    count = count + 1 - jnp.minimum(jnp.abs(apart), 1)
                piece_w = weights[
                    b * block_rows : (b + 1) * block_rows, k * p_len : (k + 1) * p_len
                ]
                bands.append(piece_w * count.astype(F32))
            chunk = jnp.concatenate(bands, axis=0)
            total = chunk if total is None else total + chunk
            parts.append(chunk.astype(BF16))
        flat = jnp.concatenate(parts, axis=1)
        return part, jnp.dot(flat, vals, preferred_element_type=F32), total

    def attend_all(sources):
        def one(t, carry):
            part, numer, total = attend(t, sources)
            num[part, :] = num[part, :] + numer
            tot[part, :] = tot[part, :] + total
            return carry

        lax.fori_loop(0, tiles, one, 0)

    def both_sides(step, i):
        return [(ring_id(pos - step), i), (ring_id(pos + step), i)]

    attend_all([(st, i) for i in range(owned)])

    def full_step(step, carry):
        for i in range(owned):
            tick(step, i, False)
            attend_all(both_sides(step - 1, i))
        return carry

    lax.fori_loop(2, half_n - 1, full_step, 0)
    for i in range(owned):
        tick(half_n - 1, i, True)
        attend_all(both_sides(half_n - 2, i))
    for i in range(owned):
        attend_all(both_sides(half_n - 1, i))
    for i in range(owned):
        arrived(0, half_n, i, True)
        arrived(1, half_n, i, True)

    def att_remote(k, t, mate, slot):
        ref = att.at[slot, pl.ds(pl.multiple_of(t * TILE, TILE), TILE)]
        return pltpu.make_async_remote_copy(
            src_ref=ref,
            dst_ref=ref,
            send_sem=att_send.at[k, t],
            recv_sem=att_recv.at[k, t],
            device_id={"tp": mate},
            device_id_type=MESH,
        )

    opposite = ring_id(pos + half_n)

    def last_tile(t, carry):
        part, numer, total = attend(t, [(opposite, i) for i in range(owned)])
        below = jnp.sum(tot[part, :] + total, axis=-1, keepdims=True)
        att[tp, part, :] = ((num[part, :] + numer) / below).astype(BF16)
        att_remote(0, t, far_mate, tp).start()
        att_remote(1, t, core_mate, tp).start()
        return carry

    lax.fori_loop(0, tiles, last_tile, 0)

    wc_copy.wait()
    for k in range(3):
        wc_remote(k, mates[k], mates[k]).wait_recv()

    def finish(t):
        att_remote(1, t, core_mate, core_mate).wait_recv()
        att_remote(2, t, core_mate, far_core).wait_recv()
        part = pl.ds(pl.multiple_of(t * TILE, TILE), TILE)
        cross = None
        for h in range(tp_size):
            term = jnp.dot(att[h, part, :], wc[h], preferred_element_type=F32)
            cross = term if cross is None else cross + term
        out_v[part, :] = (pool[part, :] + gate[part, :] * cross).astype(BF16)

    def exchange(t, carry):
        att_remote(0, t, far_mate, far_mate).wait_recv()
        att_remote(2, t, core_mate, far_mate).start()

        @pl.when(t > 0)
        def _():
            finish(t - 1)

        return carry

    lax.fori_loop(0, tiles, exchange, 0)
    finish(tiles - 1)

    for k in range(3):
        wc_remote(k, mates[k], tp).wait_send()

    def sent(step, carry):
        for i in range(owned):
            piece(0, step, i, False).wait_send()
            piece(1, step, i, False).wait_send()
        return carry

    lax.fori_loop(1, half_n, sent, 0)
    for i in range(owned):
        piece(0, half_n, i, True).wait_send()
        piece(1, half_n, i, True).wait_send()
    for t in range(tiles):
        att_remote(0, t, far_mate, tp).wait_send()
        att_remote(1, t, core_mate, tp).wait_send()
        att_remote(2, t, core_mate, far_mate).wait_send()


def solution(mesh):
    n = mesh.shape["st"]
    tp_size = mesh.shape["tp"]

    def per_device(
        tokens,
        passage_ids,
        store,
        mix_gain,
        w_query,
        w_key,
        w_value,
        w_cross_out,
        head_scale,
        w_pool_in,
        w_pool_mix,
        pool_scale,
        gate_weight,
    ):
        rows, depth = tokens.shape
        owned, p_len, _ = store.shape
        hd = w_query.shape[1]
        width = w_pool_in.shape[1]
        tiles = rows // TILE
        half_n = n // 2
        hbm = pl.BlockSpec(memory_space=pl.ANY)
        vmem = pl.BlockSpec(memory_space=pltpu.VMEM)
        smem = pl.BlockSpec(memory_space=pltpu.SMEM)
        dma = pltpu.SemaphoreType.DMA
        return pl.pallas_call(
            functools.partial(kernel, n, tp_size, hd=hd),
            out_shape=jax.ShapeDtypeStruct((rows, width), BF16),
            in_specs=[hbm, smem, hbm, vmem, hbm, hbm, hbm, hbm, smem, hbm, hbm, vmem, vmem],
            out_specs=vmem,
            scratch_shapes=[
                pltpu.VMEM((rows, depth), BF16),
                pltpu.VMEM((owned, p_len, depth), BF16),
                pltpu.VMEM((depth, 2 * hd), BF16),
                pltpu.VMEM((depth, hd + width), BF16),
                pltpu.VMEM((width, width), BF16),
                pltpu.VMEM((tp_size, hd, width), BF16),
                pltpu.VMEM((n, owned, p_len, 2 * hd), BF16),
                pltpu.VMEM((TILE, depth), BF16),
                pltpu.VMEM((TILE, 128), F32),
                pltpu.VMEM((rows, hd), BF16),
                pltpu.VMEM((rows, width), F32),
                pltpu.VMEM((rows, width), F32),
                pltpu.VMEM((rows, hd), F32),
                pltpu.VMEM((rows, p_len), F32),
                pltpu.VMEM((tp_size, rows, hd), BF16),
                dma((6,)),
                dma((tiles,)),
                dma((owned,)),
                dma((3,)),
                dma((3,)),
                dma((2, half_n, owned)),
                dma((2, half_n, owned)),
                dma((3, tiles)),
                dma((3, tiles)),
            ],
            compiler_params=pltpu.CompilerParams(
                collective_id=0,
                has_side_effects=True,
                vmem_limit_bytes=60 * 1024 * 1024,
            ),
        )(
            tokens,
            passage_ids,
            store,
            mix_gain.reshape(1, depth),
            w_query,
            w_key,
            w_value,
            w_cross_out,
            head_scale,
            w_pool_in,
            w_pool_mix,
            pool_scale.reshape(tp_size, 1, width),
            gate_weight.reshape(tp_size, 1, width),
        )

    return jax.shard_map(
        per_device,
        mesh=mesh,
        in_specs=(
            P("st", None),
            P("st", None),
            P("st", None, None),
            P(),
            P(None, "tp"),
            P(None, "tp"),
            P(None, "tp"),
            P("tp", None),
            P(),
            P(None, "tp"),
            P(),
            P(),
            P(),
        ),
        out_specs=P("st", "tp"),
        check_vma=False,
    )
```

time: 97.2 us -> 50.5 us (0.52)
  Pallas kernels: 0 us -> 44.1 us
  waiting for transfers between devices: 30.6 us -> 0 us
  matrix products: 22.4 us -> 0 us
  between operations: 14.2 us -> 0.01 us
  other arithmetic: 12.8 us -> 0 us
  local copies, waits for them, and re-layouts: 12.4 us -> 5.8 us
  starting transfers between devices: 4.27 us -> 0 us
    pallas_call x0 -> x1, Pallas kernels: none -> 44.1 us  [per_device(): pl.pallas_call(functools.partial(kernel, n, tp_size, hd=hd), out_shape=ja...]
    all_gather x2 -> x0, waiting for transfers between devices: 30.5 us -> none  [the longest x1 30.5 us: per_device(): pair_all = lax.all_gather(pair_own, 'st', axis=0, tiled=True)]
    dot_general x8 -> x0, matrix products: 22.4 us -> none  [the longest x1 7.38 us: per_device(): jnp.dot(normed, w_pool_in, preferred_element_type=jnp.float32)]
    reduce_sum x1 -> x0, other arithmetic: 5.25 us -> none  [per_device(): jnp.mean(floats * floats, axis=-1, keepdims=True) + EPSILON]
    convert_element_type x7 -> x0, other arithmetic: 4.91 us -> none  [the longest x1 3.81 us: pool_residual(): return result.reshape(row_count, chan_width).astype(jnp.bfloat16)]
    all_to_all x1 -> x0, starting transfers between devices: 4.27 us -> none  [per_device(): lax.all_to_all(w_cross_out, 'tp', split_axis=1, concat_axis=0, tiled=True)]
    gather x1 -> x0, local copies, waits for them, and re-layouts: 4.17 us -> none  [per_device(): pair_all[passage_ids.reshape(-1)]]
    reshape x1 -> x2, local copies, waits for them, and re-layouts: 0.09 us -> 2.58 us  [the longest x1 1.31 us: per_device(): mix_gain.reshape(1, depth)]
  transfers between devices with their start and end apart: 3 -> 0, of which waited for: 1 -> 0; matrix products, arithmetic and copies ran while one was open for 38% -> 0% of each run, Pallas kernels for 0% -> 0%
where the time goes in v2:
time: 50.5 us; the launch traced here: 50 us
  Pallas kernels  44.1 us (87%)
  local copies, waits for them, and re-layouts  5.8 us (11%)
    pallas_call x1, Pallas kernels, per_device(): pl.pallas_call(functools.partial(kernel, n, tp_size, hd=hd), out_shape=ja...  44.1 us
    unnamed x2, local copies, waits for them, and re-layouts  3.22 us
    reshape x1, local copies, waits for them, and re-layouts, per_device(): mix_gain.reshape(1, depth)  1.31 us
    reshape x1, local copies, waits for them, and re-layouts, per_device(): pool_scale.reshape(tp_size, 1, width)  1.27 us

profile of v2, /device:TPU:0, one launch (start us, length us, event | category | flops | bytes accessed | tf_op | source)
XLA Modules:
  0.0 50.0 jit_solution(13285873067356573560)
XLA Ops:
  0.0 1.3 %reshape.12.ps_v = bf16[4,1,256]{2,1,0:T(2,128)(2,1)} reshape(bf16[1024]{0:T(1024)(128)(2,1)} %param.24) | data formatting | bytes 4096 | tf_op jit(solution)/shard_map/reshape | solution.py:440
  1.3 1.3 %copy.15.ids_s = s32[16,4]{1,0:T(8,128)} copy(s32[16,4]{0,1:T(4,128)} %param.14) | data formatting | bytes 512 | tf_op args[1]
  2.6 1.3 %reshape.9.gain_v = bf16[1,4096]{1,0:T(2,128)(2,1)} reshape(bf16[4096]{0:T(1024)(128)(2,1)} %param.16) | data formatting | bytes 16384 | tf_op jit(solution)/shard_map/reshape | solution.py:432
  3.9 44.1 %shard_map.127 = bf16[1024,256]{1,0:T(8,128)(2,1)} custom-call(bf16[1024,4096]{1,0:T(8,128)(2,1)} %tok_h.1, s32[16,4]{1,0:T(8,128)} %copy.15.ids_s, bf16[3,128,4096]{2,1,0:T(8,128)(2,1)} %store_h.1, bf16[1,4096]{1,0:T(2,128)(2,1)} %reshape.9.gain_v, bf16[4096,128]{1,0:T(8,128)(2,1)} %wq_h.1, bf16[4096,128]{1,0:T(8,128)(2,1)} %wk_h.1, ...), custom_call_target="tpu_custom_call" | custom-call | tf_op jit(solution)/shard_map/pallas_call | solution.py:392
  48.1 1.9 %copy.18 = bf16[1024,256]{1,0:T(8,128)(2,1)} copy(bf16[1024,256]{1,0:T(8,128)(2,1)} %shard_map.127) | data formatting | bytes 1048576

commit v3 on v2

--- a/solution.py
+++ b/solution.py
@@ -35,13 +35,14 @@
     out_v,
     tok,
     store,
-    wkv,
-    wqp,
+    wk,
+    wv,
+    wq,
+    wp,
+    gain_b,
     mix,
     wc,
     kv,
-    xg,
-    rs,
     q,
     pool,
     gate,
@@ -67,7 +68,7 @@
     rows = tok.shape[0]
     tiles = rows // TILE
     width = mix.shape[0]
-    blocks, per_block = ids_s.shape
+    per_block, blocks = ids_s.shape
     block_rows = rows // blocks
     tile_blocks = TILE // block_rows
     half_rows = p_len // 2
@@ -88,8 +89,8 @@
     for target in (right, left, {"tp": core_mate}, {"tp": far_mate}, {"tp": far_core}):
         pl.semaphore_signal(barrier, inc=1, device_id=target, device_id_type=MESH)
 
-    wk_copy = pltpu.make_async_copy(wk_h, wkv.at[:, 0:hd], local_sem.at[0])
-    wv_copy = pltpu.make_async_copy(wv_h, wkv.at[:, hd : 2 * hd], local_sem.at[1])
+    wk_copy = pltpu.make_async_copy(wk_h, wk, local_sem.at[0])
+    wv_copy = pltpu.make_async_copy(wv_h, wv, local_sem.at[1])
     wk_copy.start()
     wv_copy.start()
     store_copies = [
@@ -97,8 +98,8 @@
     ]
     for copy in store_copies:
         copy.start()
-    wq_copy = pltpu.make_async_copy(wq_h, wqp.at[:, 0:hd], local_sem.at[2])
-    wp_copy = pltpu.make_async_copy(wp_h, wqp.at[:, hd : hd + width], local_sem.at[3])
+    wq_copy = pltpu.make_async_copy(wq_h, wq, local_sem.at[2])
+    wp_copy = pltpu.make_async_copy(wp_h, wp, local_sem.at[3])
     mix_copy = pltpu.make_async_copy(mix_h.at[tp], mix, local_sem.at[4])
     wq_copy.start()
     wp_copy.start()
@@ -160,11 +161,13 @@
     def head_normal(values):
         return values * lax.rsqrt(jnp.mean(values * values, axis=-1, keepdims=True) + EPSILON)
 
+    gain_b[...] = jnp.broadcast_to(gain_v[...].reshape(1, depth), (TILE, depth))
     wk_copy.wait()
     wv_copy.wait()
     for i in range(owned):
         store_copies[i].wait()
-        both = jnp.dot(store[i], wkv[...], preferred_element_type=F32)
+        pair = jnp.concatenate([wk[...], wv[...]], axis=1)
+        both = jnp.dot(store[i], pair, preferred_element_type=F32)
         kv[st, i, :, 0:hd] = head_normal(both[:, 0:hd]).astype(BF16)
         kv[st, i, :, hd : 2 * hd] = both[:, hd : 2 * hd].astype(BF16)
         if i == 0:
@@ -189,24 +192,31 @@
     band = jnp.where((gap >= 0) & (gap < window), 1.0, 0.0).astype(BF16)
     position = lax.broadcasted_iota(jnp.int32, (SEQ_LEN, width), 0)
     counted = jnp.minimum(position + 1, window).astype(F32)
-    strip = 32
+    chunk = 1024
+    scale_all = ps_v[...].astype(F32).reshape(1, tp_size * width)
+    pool_row = scale_all[:, 0:width]
+    for g in range(1, tp_size):
+        pool_row = jnp.where(tp == g, scale_all[:, g * width : (g + 1) * width], pool_row)
 
     def token_tile(t, carry):
         tok_copy(t).wait()
 
-        def norm_strip(u, carry):
-            inner = pl.ds(pl.multiple_of(u * strip, strip), strip)
-            x = tok[pl.ds(pl.multiple_of(t * TILE + u * strip, strip), strip), :]
+        part = pl.ds(pl.multiple_of(t * TILE, TILE), TILE)
+        projected = jnp.zeros((TILE, hd + width), F32)
+        squares = jnp.zeros((TILE, 128), F32)
+        for c in range(depth // chunk):
+            cols = slice(c * chunk, (c + 1) * chunk)
+            x = tok[part, cols]
             xf = x.astype(F32)
-            square = jnp.mean(xf * xf, axis=-1, keepdims=True)
-            rs[inner, :] = jnp.broadcast_to(lax.rsqrt(square + EPSILON), (strip, 128))
-            xg[inner, :] = (xf * gain_v[...]).astype(BF16)
-            return carry
-
-        lax.fori_loop(0, TILE // strip, norm_strip, 0)
-        part = pl.ds(pl.multiple_of(t * TILE, TILE), TILE)
-        scale_row = rs[:, 0:1]
-        projected = jnp.dot(xg[...], wqp[...], preferred_element_type=F32) * scale_row
+            xx = xf * xf
+            for k in range(chunk // 128):
+                squares = squares + xx[:, k * 128 : (k + 1) * 128]
+            pair = jnp.concatenate([wq[cols, :], wp[cols, :]], axis=1)
+            projected = projected + jnp.dot(
+                x * gain_b[:, cols], pair, preferred_element_type=F32
+            )
+        mean_square = jnp.sum(squares, axis=-1, keepdims=True) / depth
+        projected = projected * lax.rsqrt(mean_square + EPSILON)
         q[part, :] = head_normal(projected[:, 0:hd]).astype(BF16)
         pooled = projected[:, hd : hd + width].astype(BF16)
         for sequence in range(TILE // SEQ_LEN):
@@ -218,7 +228,7 @@
                 pl.multiple_of(t * TILE + sequence * SEQ_LEN, SEQ_LEN), SEQ_LEN
             )
             mixed = jnp.dot(residual, mix[...], preferred_element_type=F32)
-            pool[place, :] = mixed * ps_v[tp].astype(F32)
+            pool[place, :] = mixed * pool_row
             gate[place, :] = jax.nn.sigmoid(values * gw_v[tp])
         num[part, :] = jnp.zeros((TILE, hd), F32)
         tot[part, :] = jnp.zeros((TILE, p_len), F32)
@@ -249,7 +259,7 @@
             for b in range(tile_blocks):
                 count = jnp.int32(0)
                 for j in range(per_block):
-                    apart = ids_s[t * tile_blocks + b, j] - wanted
+                    apart = ids_s[j, t * tile_blocks + b] - wanted
                     count = count + 1 - jnp.minimum(jnp.abs(apart), 1)
                 piece_w = weights[
                     b * block_rows : (b + 1) * block_rows, k * p_len : (k + 1) * p_len
@@ -397,13 +407,14 @@
             scratch_shapes=[
                 pltpu.VMEM((rows, depth), BF16),
                 pltpu.VMEM((owned, p_len, depth), BF16),
-                pltpu.VMEM((depth, 2 * hd), BF16),
-                pltpu.VMEM((depth, hd + width), BF16),
+                pltpu.VMEM((depth, hd), BF16),
+                pltpu.VMEM((depth, hd), BF16),
+                pltpu.VMEM((depth, hd), BF16),
+                pltpu.VMEM((depth, width), BF16),
+                pltpu.VMEM((TILE, depth), BF16),
                 pltpu.VMEM((width, width), BF16),
                 pltpu.VMEM((tp_size, hd, width), BF16),
                 pltpu.VMEM((n, owned, p_len, 2 * hd), BF16),
-                pltpu.VMEM((TILE, depth), BF16),
-                pltpu.VMEM((TILE, 128), F32),
                 pltpu.VMEM((rows, hd), BF16),
                 pltpu.VMEM((rows, width), F32),
                 pltpu.VMEM((rows, width), F32),
@@ -427,9 +438,9 @@
             ),
         )(
             tokens,
-            passage_ids,
+            passage_ids.T,
             store,
-            mix_gain.reshape(1, depth),
+            mix_gain,
             w_query,
             w_key,
             w_value,
@@ -437,7 +448,7 @@
             head_scale,
             w_pool_in,
             w_pool_mix,
-            pool_scale.reshape(tp_size, 1, width),
+            pool_scale,
             gate_weight.reshape(tp_size, 1, width),
         )
 

time: 50.5 us -> 41.8 us (0.83)
  Pallas kernels: 44.1 us -> 39.5 us
  local copies, waits for them, and re-layouts: 5.8 us -> 1.87 us
    pallas_call x1, Pallas kernels: 44.1 us -> 39.5 us  [per_device(): pl.pallas_call(functools.partial(kernel, n, tp_size, hd=hd), out_shape=ja...]
    reshape x2 -> x0, local copies, waits for them, and re-layouts: 2.58 us -> none  [the longest x1 1.31 us: per_device(): mix_gain.reshape(1, depth)]
    unnamed x2 -> x1, local copies, waits for them, and re-layouts: 3.22 us -> 1.87 us
where the time goes in v3:
time: 41.8 us; the launch traced here: 41.4 us
  Pallas kernels  39.5 us (94%)
  local copies, waits for them, and re-layouts  1.87 us (4%)
    pallas_call x1, Pallas kernels, per_device(): pl.pallas_call(functools.partial(kernel, n, tp_size, hd=hd), out_shape=ja...  39.5 us
    unnamed x1, local copies, waits for them, and re-layouts  1.87 us

profile of v3, /device:TPU:0, one launch (start us, length us, event | category | flops | bytes accessed | tf_op | source)
XLA Modules:
  0.0 41.4 jit_solution(15901337812310041339)
XLA Ops:
  0.0 39.5 %shard_map.127 = bf16[1024,256]{1,0:T(8,128)(2,1)} custom-call(bf16[1024,4096]{1,0:T(8,128)(2,1)} %tok_h.1, s32[4,16]{1,0:T(4,128)} %bitcast.3, bf16[3,128,4096]{2,1,0:T(8,128)(2,1)} %store_h.1, bf16[4096]{0:T(1024)(128)(2,1)} %gain_v.1, bf16[4096,128]{1,0:T(8,128)(2,1)} %wq_h.1, bf16[4096,128]{1,0:T(8,128)(2,1)} %wk_h.1, bf16[4096,128]{1,0:T(8,128)(2,1)} %wv_h.1, ...), custom_call_target="tpu_custom_call" | custom-call | tf_op jit(solution)/shard_map/pallas_call | solution.py:402
  39.5 1.9 %copy.15 = bf16[1024,256]{1,0:T(8,128)(2,1)} copy(bf16[1024,256]{1,0:T(8,128)(2,1)} %shard_map.127) | data formatting | bytes 1048576
